TPU v7x, 32 devices: a whole 2x2x4 slice. The times are simulated.
32 devices in a mesh: rep: 2 (over x), fs: 8 (over z, y), tp: 2 (over core).
Axes of the slice: x: 2, y: 2, z: 4, core: 2. Of those that a mesh axis runs over, the one named last changes fastest.
Arguments:
- tokens: bfloat16 [10240, 2048], P(('rep', 'fs'), 'tp'), may hold values from -6 to 6
- norm_first: float32 [2048], replicated, may hold values from 0.1 to 1.9
- norm_mix: float32 [2048], replicated, may hold values from 0.1 to 1.9
- norm_second: float32 [2048], replicated, may hold values from 0.1 to 1.9
- gate_weight: float32 [2048, 2816], P('fs', 'tp'), may hold values from -0.125 to 0.125
- up_weight: float32 [2048, 2816], P('fs', 'tp'), may hold values from -0.125 to 0.125
- down_weight: float32 [2816, 2048], P('tp', 'fs'), may hold values from -0.109375 to 0.109375
- gate_scale: float32 [2816], P('tp'), may hold values from 0.3 to 3
- up_scale: float32 [2816], P('tp'), may hold values from 0.3 to 3
- down_scale: float32 [2048], P('fs'), may hold values from 0.3 to 3
- u_weight: float32 [2048, 1024], P('fs', 'tp'), may hold values from -0.125 to 0.125
- v_weight: float32 [2048, 1024], P('fs', 'tp'), may hold values from -0.125 to 0.125
- u_scale: float32 [1024], P('tp'), may hold values from 0.3 to 3
- v_scale: float32 [1024], P('tp'), may hold values from 0.15 to 6
- ln_gain: float32 [1024], P('tp'), may hold values from 0.1 to 1.9
- ln_bias: float32 [1024], P('tp'), may hold values from -3 to 3
- spatial_weight: bfloat16 [8, 128, 128], P('tp'), may hold values from -0.25 to 0.25
- spatial_bias: float32 [8, 128], P('tp'), may hold values from 0.1 to 1.9
- out_weight: float32 [1024, 2048], P('tp', 'fs'), may hold values from -0.1875 to 0.1875
- out_scale: float32 [2048], P('fs'), may hold values from 0.3 to 3
Outputs:
- layer_out: bfloat16 [10240, 2048], P(('rep', 'fs'), 'tp')
All inputs are finite; a program needn't handle non-finite values.
Results may differ from a plain program's by a relative error of at most 0.019.
Values may be sent and summed in bfloat16 or wider, within the bound.
No kernel may reach another device: no remote copies, remote signals or barrier semaphores. Data moves between devices by JAX's collectives and lax.ppermute only.
A program may use at most 128 MiB of HBM per device.

v0:
```python
import jax
import jax.numpy as jnp
from jax import lax
from jax.sharding import PartitionSpec as P

BW = 1024
SPAN = 128
EPS = 1e-06


def add_pair(left, pieces):
    return (
        jnp.dot(left, pieces[0], preferred_element_type=jnp.float32),
        jnp.dot(left, pieces[1], preferred_element_type=jnp.float32),
    )


def on_device(
    tokens,
    norm_first,
    norm_mix,
    norm_second,
    gate_weight,
    up_weight,
    down_weight,
    gate_scale,
    up_scale,
    down_scale,
    u_weight,
    v_weight,
    u_scale,
    v_scale,
    ln_gain,
    ln_bias,
    spatial_weight,
    spatial_bias,
    out_weight,
    out_scale,
):
    wide_scales = (
        lax.all_gather(down_scale, "fs", axis=0, tiled=True),
        lax.all_gather(out_scale, "fs", axis=0, tiled=True),
    )
    gate_low = gate_weight.astype(jnp.bfloat16)
    up_low = up_weight.astype(jnp.bfloat16)
    down_low = down_weight.astype(jnp.bfloat16)
    count = tokens.shape[0]

    def full_norm(rows, gain):
        whole = lax.all_gather(rows, "tp", axis=1, tiled=True)
        values = whole.astype(jnp.float32)
        factor = lax.rsqrt(jnp.mean(values * values, axis=1, keepdims=True) + EPS)
        return (values * factor * gain).astype(jnp.bfloat16)

    def spread_sum(term):
        return lax.psum_scatter(
            term.astype(jnp.bfloat16), "tp", scatter_dimension=1, tiled=True
        ).astype(jnp.float32)

    gate_all, up_all = (
        lax.all_gather(gate_low, "fs", axis=0, tiled=True),
        lax.all_gather(up_low, "fs", axis=0, tiled=True),
    )

    def hidden_units(normed):
        gate = jnp.dot(normed, gate_all, preferred_element_type=jnp.float32) * gate_scale
        up_part = jnp.dot(normed, up_all, preferred_element_type=jnp.float32) * up_scale
        return (jax.nn.silu(gate) * up_part).astype(jnp.bfloat16)

    first_hidden = hidden_units(full_norm(tokens, norm_first))
    down_all = lax.all_gather(down_low, "fs", axis=1, tiled=True)
    first_term = (
        jnp.dot(first_hidden, down_all, preferred_element_type=jnp.float32) * wide_scales[0]
    )
    first = spread_sum(first_term)
    middle = (tokens.astype(jnp.float32) + 0.5 * first).astype(jnp.bfloat16)
    mix_normed = full_norm(middle, norm_mix)
    u_low = u_weight.astype(jnp.bfloat16)
    v_low = v_weight.astype(jnp.bfloat16)
    u_acc, v_acc = add_pair(
        mix_normed,
        (
            lax.all_gather(u_low, "fs", axis=0, tiled=True),
            lax.all_gather(v_low, "fs", axis=0, tiled=True),
        ),
    )
    u_pre = u_acc * u_scale
    v_act = jax.nn.gelu(v_acc * v_scale, approximate=True)
    totals = lax.psum((jnp.sum(v_act, axis=1), jnp.sum(v_act * v_act, axis=1)), "tp")
    v_mean = (totals[0] / BW)[:, None]
    v_var = (totals[1] / BW)[:, None] - v_mean * v_mean
    v_normed = ((v_act - v_mean) * lax.rsqrt(v_var + EPS) * ln_gain + ln_bias).astype(jnp.bfloat16)
    local_groups = spatial_weight.shape[0]
    channels = v_act.shape[1] // local_groups
    blocks = v_normed.reshape(count // SPAN, SPAN, local_groups, channels)
    lower = jnp.tril(jnp.ones((SPAN, SPAN), jnp.bool_))
    masked = jnp.where(lower[None], spatial_weight, jnp.zeros_like(spatial_weight))
    spatial = jnp.einsum("gts,nsgc->ntgc", masked, blocks, preferred_element_type=jnp.float32)
    spatial = spatial + spatial_bias.T[None, :, :, None]
    mixed = (jax.nn.gelu(u_pre, approximate=True) * spatial.reshape(count, v_act.shape[1])).astype(
        jnp.bfloat16
    )
    out_low = out_weight.astype(jnp.bfloat16)
    mix_term = (
        jnp.dot(
            mixed,
            lax.all_gather(out_low, "fs", axis=1, tiled=True),
            preferred_element_type=jnp.float32,
        )
        * wide_scales[1]
    )
    second = (middle.astype(jnp.float32) + spread_sum(mix_term)).astype(jnp.bfloat16)
    second_hidden = hidden_units(full_norm(second, norm_second))
    last = spread_sum(
        jnp.dot(second_hidden, down_all, preferred_element_type=jnp.float32) * wide_scales[0]
    )
    return (second.astype(jnp.float32) + 0.5 * last).astype(jnp.bfloat16)


def solution(mesh):
    placed = (
        P(("rep", "fs"), "tp"),
        P(),
        P(),
        P(),
        P("fs", "tp"),
        P("fs", "tp"),
        P("tp", "fs"),
        P("tp"),
        P("tp"),
        P("fs"),
        P("fs", "tp"),
        P("fs", "tp"),
        P("tp"),
        P("tp"),
        P("tp"),
        P("tp"),
        P("tp", None, None),
        P("tp", None),
        P("tp", "fs"),
        P("fs"),
    )
    return jax.shard_map(
        on_device, mesh=mesh, in_specs=placed, out_specs=P(("rep", "fs"), "tp"), check_vma=False
    )
```

profile of v0, /device:TPU:0, one launch (start us, length us, event | category | flops | bytes accessed | tf_op | source)
XLA Modules:
  0.0 577.7 jit_solution(11312762153509955955)
XLA Ops:
  7.3 2.4 convert_element_type.87
  9.8 0.9 convert_element_type.88
  10.9 0.9 convert_element_type.90
  11.9 22.3 %all-gather = f32[8,1,256]{2,1,0:T(1,128)S(1)} all-gather(f32[1,1,256]{2,1,0:T(1,128)S(1)} %bitcast.34), channel_id=1, replica_groups=mesh['rep'=2,'fs'=8,'tp'=2] {'fs'}, dimensions={0}, use_global_device_ids=true | all-gather | bytes 9216 | tf_op jit(solution)/shard_map/all_gather | solution.py:41
  34.2 2.6 fusion
  36.9 81.8 %all-gather.14.cloned.1.call-done = bf16[2048,1408]{1,0:T(8,128)(2,1)} async-done(((bf16[256,1408]{1,0:T(8,128)(2,1)}), bf16[2048,1408]{1,0:T(8,128)(2,1)}) %all-gather.14.cloned.1.call-update) | async-done | bytes 5767184 | tf_op jit(solution)/shard_map/all_gather | solution.py:61
  118.7 8.7 %convolution_multiply_fusion.3 = f32[640,1408]{1,0:T(8,128)} fusion(bf16[2048,1408]{1,0:T(8,128)(2,1)} %all-gather.14.cloned.1.call-done, f32[1408]{0:T(1024)S(1)} %copy-done.19, bf16[640,2048]{1,0:T(8,128)(2,1)S(1)} %copy-done.4, f32[2048]{0:T(1024)S(1)} %copy-done.17, f32[640]{0:T(1024)S(1)} %add_rsqrt_fusion.3), kind=kOutput, calls=%fused_computation.23 | convolution fusion | flops 3697131520 | bytes 12009472 | tf_op jit(solution)/shard_map/dot_general | solution.py:66
  127.4 84.0 %all-gather.16.cloned.1.call-done = bf16[2048,1408]{1,0:T(8,128)(2,1)} async-done(((bf16[256,1408]{1,0:T(8,128)(2,1)}), bf16[2048,1408]{1,0:T(8,128)(2,1)}) %all-gather.16.cloned.1.call-update) | async-done | bytes 5767184 | tf_op jit(solution)/shard_map/all_gather | solution.py:62
  211.4 93.2 %all-gather.18.cloned.1.call-done = bf16[1408,2048]{1,0:T(8,128)(2,1)} async-done(((bf16[1408,256]{1,0:T(8,128)(2,1)}), bf16[1408,2048]{1,0:T(8,128)(2,1)}) %all-gather.18.cloned.1.call-update) | async-done | bytes 5767184 | tf_op jit(solution)/shard_map/all_gather | solution.py:71
  304.6 15.4 %multiply_convert_fusion.2 = bf16[640,2048]{1,0:T(8,128)(2,1)} fusion(bf16[1408,2048]{1,0:T(8,128)(2,1)} %all-gather.18.cloned.1.call-done, f32[2048]{0:T(1024)S(1)} %bitcast.30, bf16[2048,1408]{1,0:T(8,128)(2,1)} %all-gather.16.cloned.1.call-done, f32[640,1408]{1,0:T(8,128)} %convolution_multiply_fusion.3, f32[1408]{0:T(1024)S(1)} %copy-done.20, ...), kind=kOutput, calls=%fused_computation.17 | convolution fusion | flops 7396147200 | bytes 20406272 | tf_op jit(solution)/shard_map/dot_general | solution.py:73
  320.1 8.5 %reduce-scatter.4.cloned.1.call-done = bf16[640,1024]{1,0:T(8,128)(2,1)} async-done(((bf16[640,2048]{1,0:T(8,128)(2,1)}), bf16[640,1024]{1,0:T(8,128)(2,1)}) %reduce-scatter.4.cloned.1.call-update) | async-done | bytes 1310736 | tf_op jit(solution)/shard_map/reduce_scatter | solution.py:56
  328.7 2.9 add_convert_fusion.2
  331.7 0.7 convert_element_type.98
  332.5 0.7 convert_element_type.97
  334.2 21.1 %all-gather.1 = f32[8,1,256]{2,1,0:T(1,128)S(1)} all-gather(f32[1,1,256]{2,1,0:T(1,128)S(1)} %bitcast.35), channel_id=1, replica_groups=mesh['rep'=2,'fs'=8,'tp'=2] {'fs'}, dimensions={0}, use_global_device_ids=true | all-gather | bytes 9216 | tf_op jit(solution)/shard_map/all_gather | solution.py:42
  355.3 2.6 fusion.3
  357.9 38.9 %all-gather.24.cloned.1.call-done = bf16[2048,512]{1,0:T(8,128)(2,1)} async-done(((bf16[256,512]{1,0:T(8,128)(2,1)}), bf16[2048,512]{1,0:T(8,128)(2,1)}) %all-gather.24.cloned.1.call-update) | async-done | bytes 2097168 | tf_op jit(solution)/shard_map/all_gather | solution.py:84
  396.8 4.6 fusion.57
  401.4 2.6 all-reduce
  404.1 1.6 add_convert_fusion.3
  406.3 1.0 copy.26
  407.3 39.3 %all-gather.22.cloned.1.call-done = bf16[2048,512]{1,0:T(8,128)(2,1)} async-done(((bf16[256,512]{1,0:T(8,128)(2,1)}), bf16[2048,512]{1,0:T(8,128)(2,1)}) %all-gather.22.cloned.1.call-update) | async-done | bytes 2097168 | tf_op jit(solution)/shard_map/all_gather | solution.py:83
  446.6 51.0 %all-gather.26.cloned.1.call-done = bf16[512,2048]{1,0:T(8,128)(2,1)} async-done(((bf16[512,256]{1,0:T(8,128)(2,1)}), bf16[512,2048]{1,0:T(8,128)(2,1)}) %all-gather.26.cloned.1.call-update) | async-done | bytes 2097168 | tf_op jit(solution)/shard_map/all_gather | solution.py:107
  497.6 7.8 %multiply_convert_fusion.1 = bf16[640,2048]{1,0:T(8,128)(2,1)} fusion(bf16[512,2048]{1,0:T(8,128)(2,1)} %all-gather.26.cloned.1.call-done, f32[2048]{0:T(1024)S(1)} %bitcast.32, f32[80,8,4,128]{3,2,1,0:T(4,128)S(1)} %bitcast.29, bf16[2048,512]{1,0:T(8,128)(2,1)} %all-gather.22.cloned.1.call-done, bf16[640,2048]{1,0:T(8,128)(2,1)} %all-gather.20.cloned.1.call-done, ...), kind=kOutput, calls=%fused_computation.16 | convolution fusion | flops 2695823360 | bytes 10768896 | tf_op jit(solution)/shard_map/dot_general | solution.py:105
  505.4 8.6 %reduce-scatter.6.cloned.1.call-done = bf16[640,1024]{1,0:T(8,128)(2,1)} async-done(((bf16[640,2048]{1,0:T(8,128)(2,1)}), bf16[640,1024]{1,0:T(8,128)(2,1)}) %reduce-scatter.6.cloned.1.call-update) | async-done | bytes 1310736 | tf_op jit(solution)/shard_map/reduce_scatter | solution.py:56
  514.0 2.9 add_convert_fusion.1
  517.2 12.5 %all-gather.28.cloned.1.call-done = bf16[640,2048]{1,0:T(8,128)(2,1)} async-done(((bf16[640,1024]{1,0:T(8,128)(2,1)}), bf16[640,2048]{1,0:T(8,128)(2,1)}) %all-gather.28.cloned.1.call-update) | async-done | bytes 2621456 | tf_op jit(solution)/shard_map/all_gather | solution.py:50
  529.7 2.5 fusion.6
  532.2 8.7 %convolution_multiply_fusion.1 = f32[640,1408]{1,0:T(8,128)} fusion(bf16[2048,1408]{1,0:T(8,128)(2,1)} %all-gather.14.cloned.1.call-done, f32[1408]{0:T(1024)S(1)} %copy-done.19, bf16[640,2048]{1,0:T(8,128)(2,1)S(1)} %copy-done.5, f32[2048]{0:T(1024)S(1)} %copy-done.21, f32[640]{0:T(1024)S(1)} %add_rsqrt_fusion), kind=kOutput, calls=%fused_computation.20 | convolution fusion | flops 3697131520 | bytes 12009472 | tf_op jit(solution)/shard_map/dot_general | solution.py:66
  540.9 15.4 %multiply_convert_fusion = bf16[640,2048]{1,0:T(8,128)(2,1)} fusion(bf16[1408,2048]{1,0:T(8,128)(2,1)} %all-gather.18.cloned.1.call-done, f32[2048]{0:T(1024)S(1)} %bitcast.31, bf16[2048,1408]{1,0:T(8,128)(2,1)} %all-gather.16.cloned.1.call-done, f32[640,1408]{1,0:T(8,128)} %convolution_multiply_fusion.1, f32[1408]{0:T(1024)S(1)} %copy-done.20, ...), kind=kOutput, calls=%fused_computation.15 | convolution fusion | flops 7396147200 | bytes 20406272 | tf_op jit(solution)/shard_map/dot_general | solution.py:115
  556.3 11.6 %reduce-scatter.8.cloned.1.call-done = bf16[640,1024]{1,0:T(8,128)(2,1)} async-done(((bf16[640,2048]{1,0:T(8,128)(2,1)}), bf16[640,1024]{1,0:T(8,128)(2,1)}) %reduce-scatter.8.cloned.1.call-update) | async-done | bytes 1310736 | tf_op jit(solution)/shard_map/reduce_scatter | solution.py:56
  567.9 2.9 add_convert_fusion
  (82 shorter events, 3.1 us)
Async XLA Ops:
  6.5 3.3 copy-start.6
  6.5 27.7 %all-gather.12.cloned.1.call-start = ((), (), s32[]{:S(2)}) async-start(), calls=%async_computation.3 | async-start | bytes 3932160 | tf_op jit(solution)/shard_map/all_gather | solution.py:50
  7.3 3.6 copy-start.7
  7.3 111.4 %all-gather.14.cloned.1.call-start = ((), (), s32[]{:S(2)}) async-start(), calls=%async_computation.4 | async-start | bytes 6488064 | tf_op jit(solution)/shard_map/all_gather | solution.py:61
  9.8 201.6 %all-gather.16.cloned.1.call-start = ((), (), s32[]{:S(2)}) async-start(), calls=%async_computation.5 | async-start | bytes 6488064 | tf_op jit(solution)/shard_map/all_gather | solution.py:62
  10.8 107.9 %copy-start.17 = (f32[2048]{0:T(1024)S(1)}, f32[2048]{0:T(1024)}, u32[]{:S(2)}) copy-start(f32[2048]{0:T(1024)} %param.21) | copy-start | bytes 24580
  10.8 107.9 %copy-start.19 = (f32[1408]{0:T(1024)S(1)}, f32[1408]{0:T(1024)}, u32[]{:S(2)}) copy-start(f32[1408]{0:T(1024)} %param.27) | copy-start | bytes 16900
  10.8 293.8 %all-gather.18.cloned.1.call-start = ((), (), s32[]{:S(2)}) async-start(), calls=%async_computation.6 | async-start | bytes 6488064 | tf_op jit(solution)/shard_map/all_gather | solution.py:71
  11.8 316.8 %reduce-scatter.4.cloned.1.call-start = ((), (), s32[]{:S(2)}) async-start(), calls=%async_computation.7 | async-start | bytes 3932160 | tf_op jit(solution)/shard_map/reduce_scatter | solution.py:56
  34.2 84.5 %copy-start.4 = (bf16[640,2048]{1,0:T(8,128)(2,1)S(1)}, bf16[640,2048]{1,0:T(8,128)(2,1)}, u32[]{:S(2)}) copy-start(bf16[640,2048]{1,0:T(8,128)(2,1)} %all-gather.12.cloned.1.call-done) | copy-start | bytes 7864324
  36.9 267.8 %copy-start.20 = (f32[1408]{0:T(1024)S(1)}, f32[1408]{0:T(1024)}, u32[]{:S(2)}) copy-start(f32[1408]{0:T(1024)} %param.28) | copy-start | bytes 16900
  320.0 8.7 %copy-start.2 = (bf16[640,1024]{1,0:T(8,128)(2,1)S(1)}, bf16[640,1024]{1,0:T(8,128)(2,1)}, u32[]{:S(2)}) copy-start(bf16[640,1024]{1,0:T(8,128)(2,1)} %param.20) | copy-start | bytes 3932164
  320.1 11.6 %copy-start.8 = (f32[256,512]{1,0:T(8,128)S(1)}, f32[256,512]{1,0:T(8,128)}, u32[]{:S(2)}) copy-start(f32[256,512]{1,0:T(8,128)} %param.31) | copy-start | bytes 1572868
  320.1 12.5 %copy-start.9 = (f32[256,512]{1,0:T(8,128)S(1)}, f32[256,512]{1,0:T(8,128)}, u32[]{:S(2)}) copy-start(f32[256,512]{1,0:T(8,128)} %param.30) | copy-start | bytes 1572868
  320.1 35.2 %all-gather.20.cloned.1.call-start = ((), (), s32[]{:S(2)}) async-start(), calls=%async_computation.8 | async-start | bytes 3932160 | tf_op jit(solution)/shard_map/all_gather | solution.py:50
  331.6 65.2 %all-gather.24.cloned.1.call-start = ((), (), s32[]{:S(2)}) async-start(), calls=%async_computation.10 | async-start | bytes 2359296 | tf_op jit(solution)/shard_map/all_gather | solution.py:84
  332.4 64.4 %copy-start.18 = (f32[2048]{0:T(1024)S(1)}, f32[2048]{0:T(1024)}, u32[]{:S(2)}) copy-start(f32[2048]{0:T(1024)} %param.22) | copy-start | bytes 24580
  332.4 64.4 %copy-start.22 = (f32[512]{0:T(512)S(1)}, f32[512]{0:T(512)}, u32[]{:S(2)}) copy-start(f32[512]{0:T(512)} %param.33) | copy-start | bytes 6148
  332.5 114.1 %all-gather.22.cloned.1.call-start = ((), (), s32[]{:S(2)}) async-start(), calls=%async_computation.9 | async-start | bytes 2359296 | tf_op jit(solution)/shard_map/all_gather | solution.py:83
  333.3 164.3 %all-gather.26.cloned.1.call-start = ((), (), s32[]{:S(2)}) async-start(), calls=%async_computation.11 | async-start | bytes 2359296 | tf_op jit(solution)/shard_map/all_gather | solution.py:107
  334.1 179.9 %reduce-scatter.6.cloned.1.call-start = ((), (), s32[]{:S(2)}) async-start(), calls=%async_computation.12 | async-start | bytes 3932160 | tf_op jit(solution)/shard_map/reduce_scatter | solution.py:56
  355.3 41.5 %copy-start.3 = (bf16[640,2048]{1,0:T(8,128)(2,1)S(1)}, bf16[640,2048]{1,0:T(8,128)(2,1)}, u32[]{:S(2)}) copy-start(bf16[640,2048]{1,0:T(8,128)(2,1)} %all-gather.20.cloned.1.call-done) | copy-start | bytes 7864324
  357.9 46.2 %copy-start.13 = (f32[512]{0:T(512)S(1)}, f32[512]{0:T(512)}, u32[]{:S(2)}) copy-start(f32[512]{0:T(512)} %param.35) | copy-start | bytes 6148
  357.9 46.2 %copy-start.14 = (f32[512]{0:T(512)S(1)}, f32[512]{0:T(512)}, u32[]{:S(2)}) copy-start(f32[512]{0:T(512)} %param.34) | copy-start | bytes 6148
  401.4 4.4 copy-start.11
  401.4 4.5 copy-start.12
  405.9 91.7 %copy-start.23 = (f32[512]{0:T(512)S(1)}, f32[512]{0:T(512)}, u32[]{:S(2)}) copy-start(f32[512]{0:T(512)} %param.32) | copy-start | bytes 6148
  505.3 8.7 %copy-start = (bf16[640,1024]{1,0:T(8,128)(2,1)S(1)}, bf16[640,1024]{1,0:T(8,128)(2,1)}, u32[]{:S(2)}) copy-start(bf16[640,1024]{1,0:T(8,128)(2,1)} %add_convert_fusion.2) | copy-start | bytes 3932164
  505.4 24.4 %all-gather.28.cloned.1.call-start = ((), (), s32[]{:S(2)}) async-start(), calls=%async_computation.13 | async-start | bytes 3932160 | tf_op jit(solution)/shard_map/all_gather | solution.py:50
  516.9 15.3 %copy-start.21 = (f32[2048]{0:T(1024)S(1)}, f32[2048]{0:T(1024)}, u32[]{:S(2)}) copy-start(f32[2048]{0:T(1024)} %param.23) | copy-start | bytes 24580
  516.9 51.0 %reduce-scatter.8.cloned.1.call-start = ((), (), s32[]{:S(2)}) async-start(), calls=%async_computation.14 | async-start | bytes 3932160 | tf_op jit(solution)/shard_map/reduce_scatter | solution.py:56
  556.3 11.6 %copy-start.1 = (bf16[640,1024]{1,0:T(8,128)(2,1)S(1)}, bf16[640,1024]{1,0:T(8,128)(2,1)}, u32[]{:S(2)}) copy-start(bf16[640,1024]{1,0:T(8,128)(2,1)} %add_convert_fusion.1) | copy-start | bytes 3932164
  (4 other events, 8.9 us)
Sparse Core Ops, SparseCore 0:
  8.9 14.0 all-gather.11
  25.2 93.4 all-gather.13
  120.9 90.4 all-gather.15
  213.3 91.2 all-gather.17
  320.2 8.4 reduce-scatter.3
  331.8 12.6 all-gather.19
  346.5 50.2 all-gather.23
  399.0 47.6 all-gather.21
  448.7 48.8 all-gather.25
  505.5 8.4 reduce-scatter.5
  517.0 12.6 all-gather.27
  556.4 11.4 reduce-scatter.7
where the time goes:
time: 578 us
  waiting for transfers between devices  430 us (74%)
  matrix products  60.8 us (11%)
  blocking collectives  46 us (8%)
  other arithmetic  24.6 us (4%)
  between operations  13.8 us (2%)
    all_gather x1, waiting for transfers between devices, on_device(): down_all = lax.all_gather(down_low, 'fs', axis=1, tiled=True)  93.2 us
    all_gather x1, waiting for transfers between devices, on_device(): lax.all_gather(up_low, 'fs', axis=0, tiled=True)  84 us
    all_gather x1, waiting for transfers between devices, on_device(): lax.all_gather(gate_low, 'fs', axis=0, tiled=True)  81.8 us
    all_gather x1, waiting for transfers between devices, on_device(): lax.all_gather(out_low, 'fs', axis=1, tiled=True)  51 us
    all_gather x1, waiting for transfers between devices, on_device(): lax.all_gather(u_low, 'fs', axis=0, tiled=True)  39.3 us
    all_gather x1, waiting for transfers between devices, on_device(): lax.all_gather(v_low, 'fs', axis=0, tiled=True)  38.9 us
    reduce_scatter x3, waiting for transfers between devices, spread_sum(): lax.psum_scatter(term.astype(jnp.bfloat16), 'tp', scatter_dimension=1, ti...  28.7 us
    all_gather x1, blocking collectives, on_device(): lax.all_gather(down_scale, 'fs', axis=0, tiled=True)  22.3 us
  transfers between devices with their start and end apart: 12, of which 10 were waited for; matrix products, arithmetic and copies ran while one was open for 5% of the time, Pallas kernels for 0%

commit v1 on v0

--- a/solution.py
+++ b/solution.py
@@ -68,7 +68,13 @@
         return (jax.nn.silu(gate) * up_part).astype(jnp.bfloat16)
 
     first_hidden = hidden_units(full_norm(tokens, norm_first))
-    down_all = lax.all_gather(down_low, "fs", axis=1, tiled=True)
+    size = lax.axis_size("fs")
+    block, parts = (down_low, [down_low])
+    for _ in range(size - 1):
+        block = lax.ppermute(block, "fs", [(i, (i + 1) % size) for i in range(size)])
+        parts.insert(0, block)
+    flat = jnp.concatenate(parts, axis=1)
+    down_all = jnp.roll(flat, (lax.axis_index("fs") + 1) * down_low.shape[1], axis=1)
     first_term = (
         jnp.dot(first_hidden, down_all, preferred_element_type=jnp.float32) * wide_scales[0]
     )

time: 578 us -> 555 us (0.960)
  waiting for transfers between devices: 430 us -> 358 us
  blocking collectives: 46 us -> 68.3 us
  local copies, waits for them, and re-layouts: 1.29 us -> 21.9 us
    ppermute x0 -> x7, waiting for transfers between devices: none -> 166 us  [on_device(): lax.ppermute(block, 'fs', [(i, (i + 1) % size) for i in range(size)])]
    all_gather x1 -> x0, waiting for transfers between devices: 93.2 us -> none  [on_device(): down_all = lax.all_gather(down_low, 'fs', axis=1, tiled=True)]
    all_gather x1, waiting for transfers between devices: 81.8 us -> 0.01 us  [on_device(): lax.all_gather(gate_low, 'fs', axis=0, tiled=True)]
    all_gather x1, waiting for transfers between devices: 84 us -> 18.7 us  [on_device(): lax.all_gather(up_low, 'fs', axis=0, tiled=True)]
    all_gather x1, blocking collectives: 22.3 us -> 44.9 us  [on_device(): lax.all_gather(down_scale, 'fs', axis=0, tiled=True)]
    unnamed x48 -> x66, local copies, waits for them, and re-layouts: 0.15 us -> 20.8 us
  transfers between devices with their start and end apart: 12 -> 18, of which waited for: 10 -> 14; matrix products, arithmetic and copies ran while one was open for 5% -> 9% of each run, Pallas kernels for 0% -> 0%
where the time goes in v1:
time: 555 us; the launch traced here: 554 us
  waiting for transfers between devices  358 us (65%)
  blocking collectives  68.3 us (12%)
  matrix products  64.2 us (12%)
  other arithmetic  25.2 us (5%)
  local copies, waits for them, and re-layouts  21.9 us (4%)
  between operations  13.5 us (2%)
    ppermute x7, waiting for transfers between devices, on_device(): lax.ppermute(block, 'fs', [(i, (i + 1) % size) for i in range(size)])  166 us
    all_gather x1, waiting for transfers between devices, on_device(): lax.all_gather(out_low, 'fs', axis=1, tiled=True)  51 us
    all_gather x1, blocking collectives, on_device(): lax.all_gather(down_scale, 'fs', axis=0, tiled=True)  44.9 us
    all_gather x1, waiting for transfers between devices, on_device(): lax.all_gather(u_low, 'fs', axis=0, tiled=True)  41 us
    all_gather x1, waiting for transfers between devices, on_device(): lax.all_gather(v_low, 'fs', axis=0, tiled=True)  39.1 us
    reduce_scatter x3, waiting for transfers between devices, spread_sum(): lax.psum_scatter(term.astype(jnp.bfloat16), 'tp', scatter_dimension=1, ti...  28.6 us
    all_gather x1, blocking collectives, on_device(): lax.all_gather(out_scale, 'fs', axis=0, tiled=True)  20.9 us
    unnamed x66, local copies, waits for them, and re-layouts  20.8 us
  transfers between devices with their start and end apart: 18, of which 14 were waited for; matrix products, arithmetic and copies ran while one was open for 9% of the time, Pallas kernels for 0%

profile of v1, /device:TPU:0, one launch (start us, length us, event | category | flops | bytes accessed | tf_op | source)
XLA Modules:
  0.0 554.4 jit_solution(9326004618954592566)
XLA Ops:
  7.3 2.3 convert_element_type.87
  9.8 3.0 collective-permute-start
  12.8 2.3 convert_element_type.88
  15.2 16.8 %collective-permute-done = bf16[1408,256]{1,0:T(8,128)(2,1)S(1)} collective-permute-done((bf16[1408,256]{1,0:T(8,128)(2,1)S(1)}, bf16[1408,256]{1,0:T(8,128)(2,1)S(1)}, u32[]{:S(2)}, u32[]{:S(2)}) %collective-permute-start) | collective-permute-done | bytes 720928 | tf_op jit(solution)/shard_map/ppermute | solution.py:74
  32.0 33.4 %collective-permute-done.1 = bf16[1408,256]{1,0:T(8,128)(2,1)S(1)} collective-permute-done((bf16[1408,256]{1,0:T(8,128)(2,1)S(1)}, bf16[1408,256]{1,0:T(8,128)(2,1)S(1)}, u32[]{:S(2)}, u32[]{:S(2)}) %collective-permute-start.1) | collective-permute-done | bytes 720928 | tf_op jit(solution)/shard_map/ppermute | solution.py:74
  65.4 25.3 %collective-permute-done.2 = bf16[1408,256]{1,0:T(8,128)(2,1)S(1)} collective-permute-done((bf16[1408,256]{1,0:T(8,128)(2,1)S(1)}, bf16[1408,256]{1,0:T(8,128)(2,1)S(1)}, u32[]{:S(2)}, u32[]{:S(2)}) %collective-permute-start.2) | collective-permute-done | bytes 720928 | tf_op jit(solution)/shard_map/ppermute | solution.py:74
  91.6 36.3 %collective-permute-done.3 = bf16[1408,256]{1,0:T(8,128)(2,1)S(1)} collective-permute-done((bf16[1408,256]{1,0:T(8,128)(2,1)S(1)}, bf16[1408,256]{1,0:T(8,128)(2,1)S(1)}, u32[]{:S(2)}, u32[]{:S(2)}) %collective-permute-start.3) | collective-permute-done | bytes 720928 | tf_op jit(solution)/shard_map/ppermute | solution.py:74
  128.7 36.0 %collective-permute-done.4 = bf16[1408,256]{1,0:T(8,128)(2,1)S(1)} collective-permute-done((bf16[1408,256]{1,0:T(8,128)(2,1)S(1)}, bf16[1408,256]{1,0:T(8,128)(2,1)S(1)}, u32[]{:S(2)}, u32[]{:S(2)}) %collective-permute-start.4) | collective-permute-done | bytes 720928 | tf_op jit(solution)/shard_map/ppermute | solution.py:74
  165.6 18.1 %collective-permute-done.5 = bf16[1408,256]{1,0:T(8,128)(2,1)} collective-permute-done((bf16[1408,256]{1,0:T(8,128)(2,1)S(1)}, bf16[1408,256]{1,0:T(8,128)(2,1)}, u32[]{:S(2)}, u32[]{:S(2)}) %collective-permute-start.5) | collective-permute-done | bytes 720928 | tf_op jit(solution)/shard_map/ppermute | solution.py:74
  183.7 44.9 %all-gather = f32[8,1,256]{2,1,0:T(1,128)S(1)} all-gather(f32[1,1,256]{2,1,0:T(1,128)S(1)} %bitcast.32), channel_id=1, replica_groups=mesh['rep'=2,'fs'=8,'tp'=2] {'fs'}, dimensions={0}, use_global_device_ids=true | all-gather | bytes 9216 | tf_op jit(solution)/shard_map/all_gather | solution.py:41
  228.6 2.5 fusion
  251.2 9.6 %convolution_multiply_fusion.3 = f32[640,1408]{1,0:T(8,128)} fusion(bf16[2048,1408]{1,0:T(8,128)(2,1)} %all-gather.13.cloned.1.call-done, f32[1408]{0:T(1024)S(1)} %copy-done.21, bf16[640,2048]{1,0:T(8,128)(2,1)} %all-gather.11.cloned.1.call-done, f32[2048]{0:T(1024)S(1)} %copy-done.19, f32[640]{0:T(1024)S(1)} %add_rsqrt_fusion.3), kind=kOutput, calls=%fused_computation.27 | convolution fusion | flops 3697131520 | bytes 12009472 | tf_op jit(solution)/shard_map/dot_general | solution.py:66
  260.8 18.7 %all-gather.15.cloned.1.call-done = bf16[2048,1408]{1,0:T(8,128)(2,1)} async-done(((bf16[256,1408]{1,0:T(8,128)(2,1)}), bf16[2048,1408]{1,0:T(8,128)(2,1)}) %all-gather.15.cloned.1.call-update) | async-done | bytes 5767184 | tf_op jit(solution)/shard_map/all_gather | solution.py:62
  279.5 16.2 %multiply_convert_fusion.2 = bf16[640,2048]{1,0:T(8,128)(2,1)} fusion(bf16[1408,4096]{1,0:T(8,128)(2,1)} %constant_dynamic-update-slice_fusion, s32[]{:T(128)S(6)} %select_n.20, f32[2048]{0:T(1024)S(1)} %bitcast.28, bf16[2048,1408]{1,0:T(8,128)(2,1)} %all-gather.15.cloned.1.call-done, f32[640,1408]{1,0:T(8,128)} %convolution_multiply_fusion.3, ...), kind=kOutput, calls=%fused_computation.17 | convolution fusion | flops 7396147200 | bytes 20406276 | tf_op jit(solution)/shard_map/dot_general | solution.py:79
  295.9 8.4 %reduce-scatter.4.cloned.1.call-done = bf16[640,1024]{1,0:T(8,128)(2,1)} async-done(((bf16[640,2048]{1,0:T(8,128)(2,1)}), bf16[640,1024]{1,0:T(8,128)(2,1)}) %reduce-scatter.4.cloned.1.call-update) | async-done | bytes 1310736 | tf_op jit(solution)/shard_map/reduce_scatter | solution.py:56
  304.3 2.9 add_convert_fusion.2
  309.7 20.9 %all-gather.1 = f32[8,1,256]{2,1,0:T(1,128)S(1)} all-gather(f32[1,1,256]{2,1,0:T(1,128)S(1)} %bitcast.33), channel_id=1, replica_groups=mesh['rep'=2,'fs'=8,'tp'=2] {'fs'}, dimensions={0}, use_global_device_ids=true | all-gather | bytes 9216 | tf_op jit(solution)/shard_map/all_gather | solution.py:42
  330.7 2.4 fusion.3
  333.2 39.1 %all-gather.21.cloned.1.call-done = bf16[2048,512]{1,0:T(8,128)(2,1)} async-done(((bf16[256,512]{1,0:T(8,128)(2,1)}), bf16[2048,512]{1,0:T(8,128)(2,1)}) %all-gather.21.cloned.1.call-update) | async-done | bytes 2097168 | tf_op jit(solution)/shard_map/all_gather | solution.py:90
  372.3 4.4 fusion.67
  376.7 2.5 all-reduce
  381.1 41.0 %all-gather.19.cloned.1.call-done = bf16[2048,512]{1,0:T(8,128)(2,1)} async-done(((bf16[256,512]{1,0:T(8,128)(2,1)}), bf16[2048,512]{1,0:T(8,128)(2,1)}) %all-gather.19.cloned.1.call-update) | async-done | bytes 2097168 | tf_op jit(solution)/shard_map/all_gather | solution.py:89
  422.1 51.0 %all-gather.23.cloned.1.call-done = bf16[512,2048]{1,0:T(8,128)(2,1)} async-done(((bf16[512,256]{1,0:T(8,128)(2,1)}), bf16[512,2048]{1,0:T(8,128)(2,1)}) %all-gather.23.cloned.1.call-update) | async-done | bytes 2097168 | tf_op jit(solution)/shard_map/all_gather | solution.py:113
  473.0 7.8 %multiply_convert_fusion.1 = bf16[640,2048]{1,0:T(8,128)(2,1)} fusion(bf16[512,2048]{1,0:T(8,128)(2,1)} %all-gather.23.cloned.1.call-done, f32[2048]{0:T(1024)S(1)} %bitcast.30, f32[80,8,4,128]{3,2,1,0:T(4,128)S(1)} %bitcast.27, bf16[2048,512]{1,0:T(8,128)(2,1)} %all-gather.19.cloned.1.call-done, bf16[640,2048]{1,0:T(8,128)(2,1)} %all-gather.17.cloned.1.call-done, ...), kind=kOutput, calls=%fused_computation.16 | convolution fusion | flops 2695823360 | bytes 10768896 | tf_op jit(solution)/shard_map/dot_general | solution.py:111
  480.9 8.6 %reduce-scatter.6.cloned.1.call-done = bf16[640,1024]{1,0:T(8,128)(2,1)} async-done(((bf16[640,2048]{1,0:T(8,128)(2,1)}), bf16[640,1024]{1,0:T(8,128)(2,1)}) %reduce-scatter.6.cloned.1.call-update) | async-done | bytes 1310736 | tf_op jit(solution)/shard_map/reduce_scatter | solution.py:56
  489.5 2.9 add_convert_fusion.1
  492.7 12.5 %all-gather.25.cloned.1.call-done = bf16[640,2048]{1,0:T(8,128)(2,1)} async-done(((bf16[640,1024]{1,0:T(8,128)(2,1)}), bf16[640,2048]{1,0:T(8,128)(2,1)}) %all-gather.25.cloned.1.call-update) | async-done | bytes 2621456 | tf_op jit(solution)/shard_map/all_gather | solution.py:50
  505.2 2.3 fusion.6
  507.6 9.5 %convolution_multiply_fusion.1 = f32[640,1408]{1,0:T(8,128)} fusion(bf16[2048,1408]{1,0:T(8,128)(2,1)} %all-gather.13.cloned.1.call-done, f32[1408]{0:T(1024)S(1)} %copy-done.21, bf16[640,2048]{1,0:T(8,128)(2,1)} %all-gather.25.cloned.1.call-done, f32[2048]{0:T(1024)S(1)} %copy-done.23, f32[640]{0:T(1024)S(1)} %add_rsqrt_fusion), kind=kOutput, calls=%fused_computation.24 | convolution fusion | flops 3697131520 | bytes 12009472 | tf_op jit(solution)/shard_map/dot_general | solution.py:66
  517.1 16.2 %multiply_convert_fusion = bf16[640,2048]{1,0:T(8,128)(2,1)} fusion(bf16[1408,4096]{1,0:T(8,128)(2,1)} %constant_dynamic-update-slice_fusion, s32[]{:T(128)S(6)} %select_n.20, f32[2048]{0:T(1024)S(1)} %bitcast.29, bf16[2048,1408]{1,0:T(8,128)(2,1)} %all-gather.15.cloned.1.call-done, f32[640,1408]{1,0:T(8,128)} %convolution_multiply_fusion.1, ...), kind=kOutput, calls=%fused_computation.15 | convolution fusion | flops 7396147200 | bytes 20406276 | tf_op jit(solution)/shard_map/dot_general | solution.py:121
  533.3 11.6 %reduce-scatter.8.cloned.1.call-done = bf16[640,1024]{1,0:T(8,128)(2,1)} async-done(((bf16[640,2048]{1,0:T(8,128)(2,1)}), bf16[640,1024]{1,0:T(8,128)(2,1)}) %reduce-scatter.8.cloned.1.call-update) | async-done | bytes 1310736 | tf_op jit(solution)/shard_map/reduce_scatter | solution.py:56
  545.0 2.9 add_convert_fusion
  (113 shorter events, 28.6 us)
Async XLA Ops:
  6.5 222.1 %all-gather.11.cloned.1.call-start = ((), (), s32[]{:S(2)}) async-start(), calls=%async_computation.3 | async-start | bytes 3932160 | tf_op jit(solution)/shard_map/all_gather | solution.py:50
  7.3 176.5 %copy-start.17 = (f32[256]{0:T(256)S(1)}, f32[256]{0:T(256)}, u32[]{:S(2)}) copy-start(f32[256]{0:T(256)} %param.29) | copy-start | bytes 3076
  7.3 243.9 %all-gather.13.cloned.1.call-start = ((), (), s32[]{:S(2)}) async-start(), calls=%async_computation.4 | async-start | bytes 6488064 | tf_op jit(solution)/shard_map/all_gather | solution.py:61
  9.6 269.8 %all-gather.15.cloned.1.call-start = ((), (), s32[]{:S(2)}) async-start(), calls=%async_computation.5 | async-start | bytes 6488064 | tf_op jit(solution)/shard_map/all_gather | solution.py:62
  9.8 22.2 %collective-permute-start = (bf16[1408,256]{1,0:T(8,128)(2,1)S(1)}, bf16[1408,256]{1,0:T(8,128)(2,1)S(1)}, u32[]{:S(2)}, u32[]{:S(2)}) collective-permute-start(bf16[1408,256]{1,0:T(8,128)(2,1)S(1)} %convert_element_type.90), channel_id=1, source_target_pairs={{0,2},{2,4},{4,6},{6,8},{8,10},{10,12},{12,14},{14,0},{1,3},{3,5},... | collective-permute-start | bytes 2162696 | tf_op jit(solution)/shard_map/ppermute | solution.py:74
  15.2 289.1 %reduce-scatter.4.cloned.1.call-start = ((), (), s32[]{:S(2)}) async-start(), calls=%async_computation.6 | async-start | bytes 3932160 | tf_op jit(solution)/shard_map/reduce_scatter | solution.py:56
  32.0 33.4 %collective-permute-start.1 = (bf16[1408,256]{1,0:T(8,128)(2,1)S(1)}, bf16[1408,256]{1,0:T(8,128)(2,1)S(1)}, u32[]{:S(2)}, u32[]{:S(2)}) collective-permute-start(bf16[1408,256]{1,0:T(8,128)(2,1)S(1)} %collective-permute-done), channel_id=1, source_target_pairs={{0,2},{2,4},{4,6},{6,8},{8,10},{10,12},{12,14},{14,0},{1,3},{3,5},... | collective-permute-start | bytes 2162696 | tf_op jit(solution)/shard_map/ppermute | solution.py:74
  65.4 25.3 %collective-permute-start.2 = (bf16[1408,256]{1,0:T(8,128)(2,1)S(1)}, bf16[1408,256]{1,0:T(8,128)(2,1)S(1)}, u32[]{:S(2)}, u32[]{:S(2)}) collective-permute-start(bf16[1408,256]{1,0:T(8,128)(2,1)S(1)} %collective-permute-done.1), channel_id=1, source_target_pairs={{0,2},{2,4},{4,6},{6,8},{8,10},{10,12},{12,14},{14,0},{1,3},{3,5},... | collective-permute-start | bytes 2162696 | tf_op jit(solution)/shard_map/ppermute | solution.py:74
  91.6 36.3 %collective-permute-start.3 = (bf16[1408,256]{1,0:T(8,128)(2,1)S(1)}, bf16[1408,256]{1,0:T(8,128)(2,1)S(1)}, u32[]{:S(2)}, u32[]{:S(2)}) collective-permute-start(bf16[1408,256]{1,0:T(8,128)(2,1)S(1)} %collective-permute-done.2), channel_id=1, source_target_pairs={{0,2},{2,4},{4,6},{6,8},{8,10},{10,12},{12,14},{14,0},{1,3},{3,5},... | collective-permute-start | bytes 2162696 | tf_op jit(solution)/shard_map/ppermute | solution.py:74
  128.7 36.0 %collective-permute-start.4 = (bf16[1408,256]{1,0:T(8,128)(2,1)S(1)}, bf16[1408,256]{1,0:T(8,128)(2,1)S(1)}, u32[]{:S(2)}, u32[]{:S(2)}) collective-permute-start(bf16[1408,256]{1,0:T(8,128)(2,1)S(1)} %collective-permute-done.3), channel_id=1, source_target_pairs={{0,2},{2,4},{4,6},{6,8},{8,10},{10,12},{12,14},{14,0},{1,3},{3,5},... | collective-permute-start | bytes 2162696 | tf_op jit(solution)/shard_map/ppermute | solution.py:74
  165.6 18.1 %collective-permute-start.5 = (bf16[1408,256]{1,0:T(8,128)(2,1)S(1)}, bf16[1408,256]{1,0:T(8,128)(2,1)}, u32[]{:S(2)}, u32[]{:S(2)}) collective-permute-start(bf16[1408,256]{1,0:T(8,128)(2,1)S(1)} %collective-permute-done.4), channel_id=1, source_target_pairs={{0,2},{2,4},{4,6},{6,8},{8,10},{10,12},{12,14},{14,0},{1,3},{3,5},... | collective-permute-start | bytes 2162696 | tf_op jit(solution)/shard_map/ppermute | solution.py:74
  183.7 47.4 %collective-permute-start.6 = (bf16[1408,256]{1,0:T(8,128)(2,1)}, bf16[1408,256]{1,0:T(8,128)(2,1)}, u32[]{:S(2)}, u32[]{:S(2)}) collective-permute-start(bf16[1408,256]{1,0:T(8,128)(2,1)} %collective-permute-done.5), channel_id=1, source_target_pairs={{0,2},{2,4},{4,6},{6,8},{8,10},{10,12},{12,14},{14,0},{1,3},{3,5},... | collective-permute-start | bytes 2162696 | tf_op jit(solution)/shard_map/ppermute | solution.py:74
  251.2 28.3 %copy-start.22 = (f32[1408]{0:T(1024)S(1)}, f32[1408]{0:T(1024)}, u32[]{:S(2)}) copy-start(f32[1408]{0:T(1024)} %param.28) | copy-start | bytes 16900
  279.4 24.8 %copy-start.3 = (bf16[640,1024]{1,0:T(8,128)(2,1)S(1)}, bf16[640,1024]{1,0:T(8,128)(2,1)}, u32[]{:S(2)}) copy-start(bf16[640,1024]{1,0:T(8,128)(2,1)} %param.20) | copy-start | bytes 3932164
  295.7 14.1 %copy-start.18 = (f32[256]{0:T(256)S(1)}, f32[256]{0:T(256)}, u32[]{:S(2)}) copy-start(f32[256]{0:T(256)} %param.39) | copy-start | bytes 3076
  295.7 35.0 %all-gather.17.cloned.1.call-start = ((), (), s32[]{:S(2)}) async-start(), calls=%async_computation.7 | async-start | bytes 3932160 | tf_op jit(solution)/shard_map/all_gather | solution.py:50
  307.2 65.1 %copy-start.20 = (f32[2048]{0:T(1024)S(1)}, f32[2048]{0:T(1024)}, u32[]{:S(2)}) copy-start(f32[2048]{0:T(1024)} %param.22) | copy-start | bytes 24580
  307.2 65.1 %copy-start.24 = (f32[512]{0:T(512)S(1)}, f32[512]{0:T(512)}, u32[]{:S(2)}) copy-start(f32[512]{0:T(512)} %param.33) | copy-start | bytes 6148
  307.2 65.1 %all-gather.21.cloned.1.call-start = ((), (), s32[]{:S(2)}) async-start(), calls=%async_computation.9 | async-start | bytes 2359296 | tf_op jit(solution)/shard_map/all_gather | solution.py:90
  308.1 114.0 %all-gather.19.cloned.1.call-start = ((), (), s32[]{:S(2)}) async-start(), calls=%async_computation.8 | async-start | bytes 2359296 | tf_op jit(solution)/shard_map/all_gather | solution.py:89
  308.9 164.1 %all-gather.23.cloned.1.call-start = ((), (), s32[]{:S(2)}) async-start(), calls=%async_computation.10 | async-start | bytes 2359296 | tf_op jit(solution)/shard_map/all_gather | solution.py:113
  309.7 179.8 %reduce-scatter.6.cloned.1.call-start = ((), (), s32[]{:S(2)}) async-start(), calls=%async_computation.11 | async-start | bytes 3932160 | tf_op jit(solution)/shard_map/reduce_scatter | solution.py:56
  333.1 46.1 %copy-start.15 = (f32[512]{0:T(512)S(1)}, f32[512]{0:T(512)}, u32[]{:S(2)}) copy-start(f32[512]{0:T(512)} %param.35) | copy-start | bytes 6148
  333.1 46.1 %copy-start.16 = (f32[512]{0:T(512)S(1)}, f32[512]{0:T(512)}, u32[]{:S(2)}) copy-start(f32[512]{0:T(512)} %param.34) | copy-start | bytes 6148
  333.1 46.6 %copy-start.13 = (bf16[4,128,128]{2,1,0:T(8,128)(2,1)S(1)}, bf16[4,128,128]{2,1,0:T(8,128)(2,1)}, u32[]{:S(2)}) copy-start(bf16[4,128,128]{2,1,0:T(8,128)(2,1)} %param.36) | copy-start | bytes 393220
  333.1 46.6 %copy-start.14 = (f32[4,128]{1,0:T(4,128)S(1)}, f32[4,128]{1,0:T(4,128)}, u32[]{:S(2)}) copy-start(f32[4,128]{1,0:T(4,128)} %param.37) | copy-start | bytes 6148
  379.2 93.8 %copy-start.25 = (f32[512]{0:T(512)S(1)}, f32[512]{0:T(512)}, u32[]{:S(2)}) copy-start(f32[512]{0:T(512)} %param.32) | copy-start | bytes 6148
  473.0 16.5 %copy-start.1 = (bf16[640,1024]{1,0:T(8,128)(2,1)S(1)}, bf16[640,1024]{1,0:T(8,128)(2,1)}, u32[]{:S(2)}) copy-start(bf16[640,1024]{1,0:T(8,128)(2,1)} %add_convert_fusion.2) | copy-start | bytes 3932164
  480.9 26.7 %copy-start.23 = (f32[2048]{0:T(1024)S(1)}, f32[2048]{0:T(1024)}, u32[]{:S(2)}) copy-start(f32[2048]{0:T(1024)} %param.23) | copy-start | bytes 24580
  480.9 24.3 %all-gather.25.cloned.1.call-start = ((), (), s32[]{:S(2)}) async-start(), calls=%async_computation.12 | async-start | bytes 3932160 | tf_op jit(solution)/shard_map/all_gather | solution.py:50
  492.4 52.6 %reduce-scatter.8.cloned.1.call-start = ((), (), s32[]{:S(2)}) async-start(), calls=%async_computation.13 | async-start | bytes 3932160 | tf_op jit(solution)/shard_map/reduce_scatter | solution.py:56
  517.1 27.9 %copy-start.2 = (bf16[640,1024]{1,0:T(8,128)(2,1)S(1)}, bf16[640,1024]{1,0:T(8,128)(2,1)}, u32[]{:S(2)}) copy-start(bf16[640,1024]{1,0:T(8,128)(2,1)} %add_convert_fusion.1) | copy-start | bytes 3932164
  (12 other events, 73.9 us)
Sparse Core Ops, SparseCore 0:
  8.9 14.0 all-gather.10
  25.2 133.6 all-gather.12
  161.0 118.3 all-gather.14
  295.8 8.4 reduce-scatter.3
  307.3 12.6 all-gather.16
  322.0 50.2 all-gather.20
  374.4 47.6 all-gather.18
  424.1 48.8 all-gather.22
  481.0 8.4 reduce-scatter.5
  492.6 12.6 all-gather.24
  533.5 11.4 reduce-scatter.7
